TPU v7x, 32 devices: a whole 2x2x4 slice. The times are simulated.
32 devices in a mesh: sp: 4 (over z), dp: 8 (over y, x, core).
Axes of the slice: x: 2, y: 2, z: 4, core: 2. Of those that a mesh axis runs over, the one named last changes fastest.
Arguments:
- queries: bfloat16 [8, 512, 1024], P('dp', 'sp'), may hold values from -300 to 300
- keys: bfloat16 [8, 512, 1024], P('dp', 'sp'), may hold values from -7 to 7
- values: bfloat16 [8, 512, 1024], P('dp', 'sp'), may hold values from -6 to 6
- cum_gates: float32 [8, 16, 512], P('dp', 'sp'), may hold values from -67 to 0, as said below
- out_weight: bfloat16 [1024, 2048], P(None, 'dp'), may hold values from -0.1875 to 0.1875
Outputs:
- mixed: bfloat16 [8, 512, 2048], P('dp', 'sp')
Inputs may be any that keep to these rules, and one draw needn't show every extreme that they name: `cum_gates`: never rises along positions.
All inputs are finite; a program needn't handle non-finite values.
Results may differ from a plain program's by a relative error of at most 0.011.
Values may be sent and summed in bfloat16 or wider, within the bound.
A program may use at most 64 MiB of HBM per device.

v0:
```python
import functools

import jax
import jax.numpy as jnp
from jax import lax
from jax.experimental import pallas as pl
from jax.experimental.pallas import tpu as pltpu
from jax.sharding import PartitionSpec as P


def attend_heads(query_loc, key_loc, value_loc, cum_loc):
    length = query_loc.shape[0]
    head_count = cum_loc.shape[0]
    head_size = query_loc.shape[1] // head_count
    query_heads = query_loc.reshape(length, head_count, head_size).transpose(1, 0, 2)
    key_heads = key_loc.reshape(length, head_count, head_size).transpose(1, 0, 2)
    value_heads = value_loc.reshape(length, head_count, head_size).transpose(1, 0, 2)
    block_rows = min(512, length)
    block_count = length // block_rows
    query_blocks = query_heads.reshape(head_count, block_count, block_rows, head_size).transpose(
        1, 0, 2, 3
    )
    cum_blocks = cum_loc.reshape(head_count, block_count, block_rows).transpose(1, 0, 2)
    key_pos = jnp.arange(length)
    score_scale = head_size ** (-0.5)

    def one_block(packed):
        query_block, cum_block, block_index = packed
        scores = (
            jnp.einsum("hqd,hkd->hqk", query_block, key_heads, preferred_element_type=jnp.float32)
            * score_scale
        )
        scores = scores + cum_block[:, :, None] - cum_loc[:, None, :]
        query_pos = block_index * block_rows + jnp.arange(block_rows)
        scores = jnp.where(key_pos[None, :] <= query_pos[:, None], scores, -jnp.inf)
        row_max = jnp.max(scores, axis=-1, keepdims=True)
        expon = jnp.exp(scores - row_max)
        weights = (expon / jnp.sum(expon, axis=-1, keepdims=True)).astype(jnp.bfloat16)
        return jnp.einsum(
            "hqk,hkd->hqd", weights, value_heads, preferred_element_type=jnp.float32
        ).astype(jnp.bfloat16)

    results = lax.map(one_block, (query_blocks, cum_blocks, jnp.arange(block_count)))
    return results.transpose(0, 2, 1, 3).reshape(length, head_count * head_size)


def shards(queries, keys, values, cum_gates, out_weight):
    query_loc, key_loc, value_loc = (
        lax.all_to_all(queries[0], "sp", split_axis=1, concat_axis=0, tiled=True),
        lax.all_to_all(keys[0], "sp", split_axis=1, concat_axis=0, tiled=True),
        lax.all_to_all(values[0], "sp", split_axis=1, concat_axis=0, tiled=True),
    )
    head_out = attend_heads(query_loc, key_loc, value_loc, cum_gates[0])
    token_rows = lax.all_to_all(head_out, "sp", split_axis=0, concat_axis=1, tiled=True)
    mixed_rows = jnp.dot(
        token_rows,
        lax.all_gather(out_weight, "dp", axis=1, tiled=True),
        preferred_element_type=jnp.float32,
    )
    return mixed_rows.astype(jnp.bfloat16)[None]


MESH = pl.DeviceIdType.MESH
LANES = 128
HUB = 1


def flip(index, bit):
    return index + bit - 2 * bit * (lax.div(index, bit) % 2)


def head_pair(q, ks, vs, gates, first_key, row_block, scale, head_size, causal):
    rows = q.shape[0]
    even = lax.broadcasted_iota(jnp.int32, (rows, LANES), 1) < head_size
    q = q * jnp.asarray(scale, q.dtype)
    zero = jnp.zeros_like(q)
    stacked = jnp.concatenate([jnp.where(even, q, zero), jnp.where(even, zero, q)], axis=0)
    k = ks[0] if len(ks) == 1 else jnp.concatenate(ks, axis=0)
    v = vs[0] if len(vs) == 1 else jnp.concatenate(vs, axis=0)
    span = k.shape[0]
    scores = lax.dot_general(
        stacked, k, (((1,), (1,)), ((), ())), preferred_element_type=jnp.float32
    )
    key_gates = gates[:, pl.ds(pl.multiple_of(first_key * rows, LANES), span)]
    row_gates = gates[:, pl.ds(pl.multiple_of(row_block * rows, LANES), rows)].T
    parts = []
    for n in range(2):
        part = scores[n * rows : (n + 1) * rows] + (
            row_gates[:, 8 * n : 8 * n + 1] - key_gates[8 * n : 8 * n + 1]
        )
        if causal:
            row = lax.broadcasted_iota(jnp.int32, (rows, span), 0) + (span - rows)
            col = lax.broadcasted_iota(jnp.int32, (rows, span), 1)
            part = jnp.where(col <= row, part, -jnp.inf)
        parts.append(part)
    tops = [jnp.max(part, axis=1, keepdims=True) for part in parts]
    probs = jnp.concatenate(
        [jnp.exp(part - top).astype(v.dtype) for part, top in zip(parts, tops)], axis=0
    )
    wide = jnp.concatenate([v, jnp.ones((span, LANES), v.dtype)], axis=1)
    sums = jnp.dot(probs, wide, preferred_element_type=jnp.float32)
    total = jnp.where(even, sums[:rows, LANES:], sums[rows:, LANES:])
    result = jnp.where(even, sums[:rows, :LANES], sums[rows:, :LANES]) / total
    top = jnp.where(even, tops[0], tops[1])
    return result, top + jnp.log(total)


def layer_kernel(
    sizes, q_hbm, k_hbm, v_hbm, g_hbm, w_hbm, out_ref,
    q_own, q_in, k_buf, v_buf, g_in, g_pair, o_out, s_out, o_in, s_in, o_own, s_own, heads, w_buf,
    q_ss, q_rs, kv_ss, kv_rs, o_ss, o_rs, s_ss, s_rs, g_ss, g_rs, w_ss, w_rs, loc, seen_sem,
):
    sp, chunks, head_size, scale = sizes
    z, d = lax.axis_index("sp"), lax.axis_index("dp")
    rows = q_own.shape[0]
    half = w_buf.shape[1] // 2
    core, xs, ys = flip(d, 1), flip(d, 2), flip(d, 4)

    def cols(c):
        return pl.ds(pl.multiple_of(c * LANES, LANES), LANES)

    def remote(src, dst, ss, rs, **device):
        return pltpu.make_async_remote_copy(
            src_ref=src, dst_ref=dst, send_sem=ss, recv_sem=rs,
            device_id=device, device_id_type=MESH,
        )

    local = [
        pltpu.make_async_copy(q_hbm.at[0], q_own, loc.at[0]),
        pltpu.make_async_copy(k_hbm.at[0], k_buf.at[1], loc.at[1]),
        pltpu.make_async_copy(v_hbm.at[0], v_buf.at[1], loc.at[2]),
        pltpu.make_async_copy(g_hbm.at[0], g_in.at[z], loc.at[3]),
        pltpu.make_async_copy(w_hbm, w_buf.at[0], loc.at[4]),
    ]
    for copy in local:
        copy.start()

    barrier = pltpu.get_barrier_semaphore()
    @pl.when(z > 0)
    def _():
        pl.semaphore_signal(barrier, inc=1, device_id={"sp": z - 1}, device_id_type=MESH)

    @pl.when(z < sp - 1)
    def _():
        pl.semaphore_signal(barrier, inc=1, device_id={"sp": z + 1}, device_id_type=MESH)

    for peer in (core, xs, ys):
        pl.semaphore_signal(barrier, inc=1, device_id={"dp": peer}, device_id_type=MESH)
    pl.semaphore_wait(
        barrier, 3 + (z > 0).astype(jnp.int32) + (z < sp - 1).astype(jnp.int32)
    )

    for teller, pair in ((HUB + 1, (HUB, HUB + 2)), (HUB, (HUB - 1, HUB + 1))):
        @pl.when(z == teller)
        def _():
            for target in pair:
                pl.semaphore_signal(
                    seen_sem.at[teller - HUB], inc=1, device_id={"sp": target},
                    device_id_type=MESH,
                )

    def gate_copy(owner, target, relayed=0):
        return remote(
            g_in.at[owner], g_in.at[owner], g_ss.at[relayed, target], g_rs.at[owner], sp=target
        )

    def gate_sends(run):
        for owner, target in ((0, 1), (1, 0), (1, 2), (2, 1), (2, 3), (3, 2)):
            @pl.when(z == owner)
            def _():
                run(gate_copy(owner, target))

    def q_copy(c, slot, way, target):
        return remote(
            q_own.at[:, cols(c)], q_in.at[slot, :, cols(c)],
            q_ss.at[way, c], q_rs.at[slot, c], sp=target,
        )

    def k_copy(c):
        return remote(
            k_buf.at[1, :, cols(c)], k_buf.at[0, :, cols(c)],
            kv_ss.at[0, c], kv_rs.at[0, c], sp=HUB,
        )

    def v_copy(c):
        return remote(
            v_buf.at[1, :, cols(c)], v_buf.at[0, :, cols(c)],
            kv_ss.at[1, c], kv_rs.at[1, c], sp=HUB,
        )

    def w_copy(number, slot, part, bit, peer):
        span = pl.ds(part * half, half)
        return remote(
            w_buf.at[slot, span], w_buf.at[slot ^ bit, span], w_ss.at[number], w_rs.at[slot ^ bit, part], dp=peer
        )

    w_plan = {
        "first": [(0, 0, 0, 2, xs), (1, 0, 1, 4, ys), (2, 0, 1, 2, xs), (3, 0, 0, 4, ys),
                  (4, 0, 0, 1, core), (5, 0, 1, 1, core)],
        "early": [(6, 2, 0, 4, ys), (7, 4, 1, 2, xs), (8, 2, 0, 1, core), (9, 4, 1, 1, core)],
        "middle": [(10, 2, 1, 1, core), (11, 4, 0, 1, core)],
        "late": [(12, 6, 0, 1, core), (13, 6, 1, 1, core)],
    }

    def w_arrived(slot, part):
        span = pl.ds(part * half, half)
        remote(
            w_hbm.at[span], w_buf.at[slot, span], w_ss.at[0], w_rs.at[slot, part], dp=core
        ).wait_recv()

    def relay(stage):
        seen = []
        for number, slot, part, bit, peer in w_plan[stage]:
            if slot and (slot, part) not in seen:
                w_arrived(slot, part)
                seen.append((slot, part))
            w_copy(number, slot, part, bit, peer).start()

    local[4].wait()
    relay("first")
    for copy in local[:3]:
        copy.wait()

    local[3].wait()
    gate_sends(lambda copy: copy.start())

    @pl.when(z == 0)
    def _():
        for c in range(chunks):
            k_copy(c).start()
            v_copy(c).start()
            if c == 0:
                pl.semaphore_wait(seen_sem.at[0], 1)
                gate_copy(0, 2).start()

    @pl.when(z == HUB + 1)
    def _():
        for c in range(chunks):
            q_copy(c, 0, 0, HUB).start()
            if c == 0:
                pl.semaphore_wait(seen_sem.at[0], 1)
                gate_copy(2, 0).start()

    @pl.when(z == HUB + 2)
    def _():
        q_copy(0, 1, 1, HUB + 1).start()
        pl.semaphore_wait(seen_sem.at[1], 1)
        gate_copy(3, 1).start()
        q_copy(0, 1, 0, HUB).start()
        q_copy(1, 1, 0, HUB).start()
        for c in range(1, chunks):
            q_copy(c, 1, 1, HUB + 1).start()
            if c + 1 < chunks:
                q_copy(c + 1, 1, 0, HUB).start()

    @pl.when(z == HUB)
    def _():
        pl.semaphore_wait(seen_sem.at[1], 1)
        gate_copy(1, 3).start()

    for owner in range(sp):
        @pl.when(z != owner)
        def _():
            gate_copy(owner, (owner + 1) % sp).wait_recv()

    @pl.when(z == HUB)
    def _():
        gate_copy(0, 3, 1).start()
        gate_copy(3, 0, 1).start()

    per = g_in.shape[1]
    for c in range(chunks):
        for n in range(2):
            head = 2 * c + n
            line = g_in[head // per, head % per : head % per + 1, :]
            g_pair[c, 8 * n : 8 * n + 8, :] = jnp.broadcast_to(line, (8, line.shape[1]))
    def attend(c, q, slots, first_key, row_block, causal):
        return head_pair(
            q[:, cols(c)], [k_buf[s, :, cols(c)] for s in slots],
            [v_buf[s, :, cols(c)] for s in slots],
            g_pair.at[c], first_key, row_block, scale, head_size, causal,
        )

    def put(c, slot, result, lse):
        o_out[slot, :, cols(c)] = result.astype(o_out.dtype)
        turned = lse.T
        s_out[slot, c, 0:8, :] = turned[0:8]
        s_out[slot, c, 8:16, :] = turned[head_size : head_size + 8]

    def o_copy(c, slot, into, target):
        return remote(
            o_out.at[slot, :, cols(c)], o_in.at[into, :, cols(c)],
            o_ss.at[slot, c], o_rs.at[into, c], sp=target,
        )

    def s_copy(c, slot, into, target):
        return remote(
            s_out.at[slot, c], s_in.at[into, c], s_ss.at[slot, c], s_rs.at[into, c], sp=target
        )

    def give(c, slot, into, target):
        s_copy(c, slot, into, target).start()
        o_copy(c, slot, into, target).start()

    def early(c):
        @pl.when(c == chunks // 2)
        def _():
            relay("early")

    @pl.when(z == 0)
    def _():
        @pl.loop(0, chunks)
        def _(c):
            early(c)
            result, _lse = attend(c, q_own, [1], z, z, True)
            heads[:, cols(c)] = result.astype(heads.dtype)

    @pl.when(z == HUB)
    def _():
        @pl.loop(0, chunks)
        def _(c):
            early(c)
            k_copy(c).wait_recv()
            v_copy(c).wait_recv()
            q_copy(c, 1, 0, HUB).wait_recv()
            put(c, 1, *attend(c, q_in.at[1], [0, 1], 0, HUB + 2, False))
            q_copy(c, 0, 0, HUB).wait_recv()
            put(c, 0, *attend(c, q_in.at[0], [0, 1], 0, HUB + 1, False))
            give(c, 1, 0, HUB + 2)
            result, _lse = attend(c, q_own, [0, 1], 0, z, True)
            heads[:, cols(c)] = result.astype(heads.dtype)
            give(c, 0, 0, HUB + 1)

    @pl.when(z > HUB)
    def _():
        @pl.loop(0, chunks)
        def _(c):
            early(c)

            @pl.when(z == HUB + 1)
            def _():
                q_copy(c, 1, 1, HUB + 1).wait_recv()
                put(c, 1, *attend(c, q_in.at[1], [1], z, HUB + 2, False))

            result, lse = attend(c, q_own, [1], z, z, True)
            o_own[:, cols(c)] = result
            s_own[:, cols(c)] = lse

            @pl.when(z == HUB + 1)
            def _():
                give(c, 1, 1, HUB + 2)

    def taken(c, into):
        s_copy(c, 0, into, HUB).wait_recv()
        o_copy(c, 0, into, HUB).wait_recv()
        turned = s_in[into, c].T
        even = lax.broadcasted_iota(jnp.int32, (rows, LANES), 1) < head_size
        lse = jnp.where(even, turned[:, 0:1], turned[:, 8:9])
        return o_in[into, :, cols(c)].astype(jnp.float32), lse

    def merge(first, second):
        (a, la), (b, lb) = first, second
        top = jnp.maximum(la, lb)
        wa, wb = jnp.exp(la - top), jnp.exp(lb - top)
        total = wa + wb
        return (a * wa + b * wb) / total, top + jnp.log(total)

    @pl.when(z <= HUB)
    def _():
        relay("middle")

    @pl.when(z > HUB)
    def _():
        @pl.loop(0, chunks)
        def _(c):
            @pl.when(c == chunks // 2 + 1)
            def _():
                relay("middle")

            @pl.when(z == HUB + 2)
            def _():
                result, lse = merge((o_own[:, cols(c)], s_own[:, cols(c)]), taken(c, 1))
                o_own[:, cols(c)] = result
                s_own[:, cols(c)] = lse

            result, _lse = merge((o_own[:, cols(c)], s_own[:, cols(c)]), taken(c, 0))
            heads[:, cols(c)] = result.astype(heads.dtype)

        relay("late")

    width = w_buf.shape[2]

    def project(slot):
        owner = d
        for bit in (1, 2, 4):
            if slot & bit:
                owner = flip(owner, bit)
        block = jnp.dot(heads[...], w_buf[slot], preferred_element_type=jnp.float32)
        out_ref[0, :, pl.ds(pl.multiple_of(owner * width, LANES), width)] = block.astype(
            out_ref.dtype
        )

    project(0)
    for part in range(2):
        w_arrived(1, part)
    project(1)
    project(2)
    project(4)
    for slot in (3, 5):
        for part in range(2):
            w_arrived(slot, part)
        project(slot)

    @pl.when(z <= HUB)
    def _():
        relay("late")

    project(6)
    for part in range(2):
        w_arrived(7, part)
    project(7)

    gate_sends(lambda copy: copy.wait_send())
    for owner, target, relayed in ((0, 2, 0), (2, 0, 0), (1, 3, 0), (3, 1, 0), (0, 3, 1), (3, 0, 1)):
        @pl.when(z == (HUB if relayed else owner))
        def _():
            gate_copy(owner, target, relayed).wait_send()

    for stage in w_plan.values():
        for entry in stage:
            w_copy(*entry).wait_send()

    @pl.when(z == 0)
    def _():
        for c in range(chunks):
            k_copy(c).wait_send()
            v_copy(c).wait_send()

    @pl.when(z > HUB)
    def _():
        for c in range(chunks):
            q_copy(c, 0, 0, HUB).wait_send()

    @pl.when(z == HUB + 2)
    def _():
        for c in range(chunks):
            q_copy(c, 1, 1, HUB + 1).wait_send()

    @pl.when((z == HUB) | (z == HUB + 1))
    def _():
        for c in range(chunks):
            s_copy(c, 1, 0, HUB + 2).wait_send()
            o_copy(c, 1, 0, HUB + 2).wait_send()

    @pl.when(z == HUB)
    def _():
        for c in range(chunks):
            s_copy(c, 0, 0, HUB + 1).wait_send()
            o_copy(c, 0, 0, HUB + 1).wait_send()


def fused_shards(sp, queries, keys, values, cum_gates, out_weight):
    _, rows, width = queries.shape
    _, per, length = cum_gates.shape
    head_size = width // (per * sp)
    depth, block = out_weight.shape
    dp = 8
    chunks = width // LANES
    bf16, f32 = queries.dtype, jnp.float32
    dma = pltpu.SemaphoreType.DMA
    return pl.pallas_call(
        functools.partial(layer_kernel, (sp, chunks, head_size, head_size ** (-0.5))),
        out_shape=jax.ShapeDtypeStruct((1, rows, block * dp), bf16),
        in_specs=[pl.BlockSpec(memory_space=pltpu.HBM)] * 5,
        out_specs=pl.BlockSpec(memory_space=pltpu.VMEM),
        scratch_shapes=[
            pltpu.VMEM((rows, width), bf16),
            pltpu.VMEM((2, rows, width), bf16),
            pltpu.VMEM((2, rows, width), bf16),
            pltpu.VMEM((2, rows, width), bf16),
            pltpu.VMEM((sp, per, length), f32),
            pltpu.VMEM((chunks, 16, length), f32),
            pltpu.VMEM((2, rows, width), bf16),
            pltpu.VMEM((2, chunks, 16, LANES), f32),
            pltpu.VMEM((2, rows, width), bf16),
            pltpu.VMEM((2, chunks, 16, LANES), f32),
            pltpu.VMEM((rows, width), f32),
            pltpu.VMEM((rows, width), f32),
            pltpu.VMEM((rows, width), bf16),
            pltpu.VMEM((dp, depth, block), bf16),
            dma((2, chunks)), dma((2, chunks)), dma((2, chunks)), dma((2, chunks)),
            dma((2, chunks)), dma((2, chunks)), dma((2, chunks)), dma((2, chunks)),
            dma((2, sp)), dma((sp,)), dma((14,)), dma((dp, 2)), dma((5,)),
            pltpu.SemaphoreType.REGULAR((2,)),
        ],
        compiler_params=pltpu.CompilerParams(collective_id=0, has_side_effects=True, vmem_limit_bytes=16 * 2**20),
        name="layer",
    )(*(pltpu.with_memory_space_constraint(x, pltpu.HBM) for x in (queries, keys, values, cum_gates, out_weight)))


def route(sp, dp, queries, keys, values, cum_gates, out_weight):
    _, rows, width = queries.shape
    head_size = width // (cum_gates.shape[1] * sp)
    fits = (
        sp == HUB + 3
        and dp == 8
        and rows == LANES
        and 2 * head_size == LANES
        and width % LANES == 0
        and out_weight.shape[1] % LANES == 0
    )
    if fits:
        return fused_shards(sp, queries, keys, values, cum_gates, out_weight)
    return shards(queries, keys, values, cum_gates, out_weight)


def solution(mesh):
    in_specs = (
        P("dp", "sp", None),
        P("dp", "sp", None),
        P("dp", "sp", None),
        P("dp", "sp", None),
        P(None, "dp"),
    )
    out_specs = P("dp", "sp", None)
    body = functools.partial(route, mesh.shape["sp"], mesh.shape["dp"])
    return jax.shard_map(body, mesh=mesh, in_specs=in_specs, out_specs=out_specs, check_vma=False)
```

profile of v0, /device:TPU:19, one launch (start us, length us, event | category | flops | bytes accessed | tf_op | source)
XLA Modules:
  0.0 28.2 jit_solution(2581309600854539350)
XLA Ops:
  0.0 27.4 %layer.1 = bf16[1,128,2048]{2,1,0:T(8,128)(2,1)S(1)} custom-call(bf16[1,128,1024]{2,1,0:T(8,128)(2,1)} %q_hbm.1, bf16[1,128,1024]{2,1,0:T(8,128)(2,1)} %k_hbm.1, bf16[1,128,1024]{2,1,0:T(8,128)(2,1)} %v_hbm.1, f32[1,4,512]{2,1,0:T(4,128)} %g_hbm.1, bf16[1024,256]{1,0:T(8,128)(2,1)} %w_hbm.1), custom_call_target="tpu_custom_call" | custom-call | tf_op jit(solution)/shard_map/layer/pallas_call | solution.py:471
  27.4 0.8 %copy.7 = bf16[1,128,2048]{2,1,0:T(8,128)(2,1)} copy(bf16[1,128,2048]{2,1,0:T(8,128)(2,1)S(1)} %layer.1) | data formatting | bytes 1048576
where the time goes:
time: 28.4 us; the launch traced here: 28.2 us
  Pallas kernels  27.4 us (96%)
  local copies, waits for them, and re-layouts  0.8 us (3%)
    pallas_call x1, Pallas kernels, fused_shards(): pl.pallas_call(functools.partial(layer_kernel, (sp, chunks, head_size, he...  27.4 us
    unnamed x1, local copies, waits for them, and re-layouts  0.8 us

commit v1 on v0

v1 whole, which is shorter than its diff:
```python
import functools

import jax
import jax.numpy as jnp
from jax import lax
from jax.experimental import pallas as pl
from jax.experimental.pallas import tpu as pltpu
from jax.sharding import PartitionSpec as P


def attend_heads(query_loc, key_loc, value_loc, cum_loc):
    length = query_loc.shape[0]
    head_count = cum_loc.shape[0]
    head_size = query_loc.shape[1] // head_count
    query_heads = query_loc.reshape(length, head_count, head_size).transpose(1, 0, 2)
    key_heads = key_loc.reshape(length, head_count, head_size).transpose(1, 0, 2)
    value_heads = value_loc.reshape(length, head_count, head_size).transpose(1, 0, 2)
    block_rows = min(512, length)
    block_count = length // block_rows
    query_blocks = query_heads.reshape(head_count, block_count, block_rows, head_size).transpose(
        1, 0, 2, 3
    )
    cum_blocks = cum_loc.reshape(head_count, block_count, block_rows).transpose(1, 0, 2)
    key_pos = jnp.arange(length)
    score_scale = head_size ** (-0.5)

    def one_block(packed):
        query_block, cum_block, block_index = packed
        scores = (
            jnp.einsum("hqd,hkd->hqk", query_block, key_heads, preferred_element_type=jnp.float32)
            * score_scale
        )
        scores = scores + cum_block[:, :, None] - cum_loc[:, None, :]
        query_pos = block_index * block_rows + jnp.arange(block_rows)
        scores = jnp.where(key_pos[None, :] <= query_pos[:, None], scores, -jnp.inf)
        row_max = jnp.max(scores, axis=-1, keepdims=True)
        expon = jnp.exp(scores - row_max)
        weights = (expon / jnp.sum(expon, axis=-1, keepdims=True)).astype(jnp.bfloat16)
        return jnp.einsum(
            "hqk,hkd->hqd", weights, value_heads, preferred_element_type=jnp.float32
        ).astype(jnp.bfloat16)

    results = lax.map(one_block, (query_blocks, cum_blocks, jnp.arange(block_count)))
    return results.transpose(0, 2, 1, 3).reshape(length, head_count * head_size)


def shards(queries, keys, values, cum_gates, out_weight):
    query_loc, key_loc, value_loc = (
        lax.all_to_all(queries[0], "sp", split_axis=1, concat_axis=0, tiled=True),
        lax.all_to_all(keys[0], "sp", split_axis=1, concat_axis=0, tiled=True),
        lax.all_to_all(values[0], "sp", split_axis=1, concat_axis=0, tiled=True),
    )
    head_out = attend_heads(query_loc, key_loc, value_loc, cum_gates[0])
    token_rows = lax.all_to_all(head_out, "sp", split_axis=0, concat_axis=1, tiled=True)
    mixed_rows = jnp.dot(
        token_rows,
        lax.all_gather(out_weight, "dp", axis=1, tiled=True),
        preferred_element_type=jnp.float32,
    )
    return mixed_rows.astype(jnp.bfloat16)[None]


MESH = pl.DeviceIdType.MESH
LANES = 128
HUB = 1
SPLIT = 32


def flip(index, bit):
    return index + bit - 2 * bit * (lax.div(index, bit) % 2)


def attend(c, qs, row_gates, k, v, key_gates, masks, scale, head_size):
    rows = qs[0].shape[0]
    span = k.shape[0]
    lane = lax.broadcasted_iota(jnp.int32, (rows, LANES), 1)
    even = lane < head_size
    picks = [jnp.where(lane % SPLIT == 2 * c + n, 1.0, 0.0).astype(k.dtype) for n in range(2)]
    wide = jnp.concatenate([k, key_gates], axis=1)
    key = lax.broadcasted_iota(jnp.int32, (span, rows), 0) - (span - rows)
    past = key <= lax.broadcasted_iota(jnp.int32, (span, rows), 1)
    scores = []
    for q in qs:
        q = q * jnp.asarray(scale, q.dtype)
        zero = jnp.zeros_like(q)
        stacked = jnp.concatenate(
            [
                jnp.concatenate([jnp.where(even, q, zero), picks[0]], axis=1),
                jnp.concatenate([jnp.where(even, zero, q), picks[1]], axis=1),
            ],
            axis=0,
        )
        scores.append(
            lax.dot_general(
                wide, stacked, (((1,), (1,)), ((), ())), preferred_element_type=jnp.float32
            )
        )
    parts = []
    for score, gate, mask in zip(scores, row_gates, masks):
        for n in range(2):
            part = score[:, n * rows : (n + 1) * rows] + gate[n : n + 1]
            parts.append(jnp.where(past, part, -jnp.inf) if mask else part)
    tops = [jnp.max(part, axis=0, keepdims=True) for part in parts]
    exps = [jnp.exp(part - top) for part, top in zip(parts, tops)]
    totals = [jnp.sum(e, axis=0, keepdims=True) for e in exps]
    results = []
    for i in range(len(qs)):
        probs = jnp.concatenate([exps[2 * i], exps[2 * i + 1]], axis=1).astype(v.dtype)
        sums = lax.dot_general(
            v, probs, (((0,), (0,)), ((), ())), preferred_element_type=jnp.float32
        )
        first = sums[:head_size, :rows] * (1.0 / totals[2 * i])
        second = sums[head_size:, rows:] * (1.0 / totals[2 * i + 1])
        lse = [tops[2 * i + n] + jnp.log(totals[2 * i + n]) for n in range(2)]
        results.append((jnp.concatenate([first, second], axis=0), jnp.concatenate(lse, axis=0)))
    return results


def layer_kernel(
    sizes, q_hbm, k_hbm, v_hbm, g_hbm, w_hbm, out_ref,
    q_own, q_in, kv_own, kv_in, g_in, g_row, g_stage, g_key, o_out, s_out, o_in, s_in, o_own, s_own,
    heads, w_buf, one_part, two_parts,
    in_rs, o_rs, snd, g_rs, g_ss, w_rs, loc, seen_sem,
):
    sp, chunks, head_size, scale = sizes
    z, d = lax.axis_index("sp"), lax.axis_index("dp")
    rows = q_own.shape[0]
    half = w_buf.shape[1] // 2
    core, xs, ys = flip(d, 1), flip(d, 2), flip(d, 4)

    def cols(c):
        return pl.ds(pl.multiple_of(c * LANES, LANES), LANES)

    def remote(src, dst, ss, rs, **device):
        return pltpu.make_async_remote_copy(
            src_ref=src, dst_ref=dst, send_sem=ss, recv_sem=rs,
            device_id=device, device_id_type=MESH,
        )

    def arrived(ref, sem):
        remote(ref, ref, snd.at[0], sem, dp=core).wait_recv()

    def sent(ref, sem):
        remote(ref, ref, sem, w_rs.at[0], dp=core).wait_send()

    local = [
        pltpu.make_async_copy(w_hbm, w_buf.at[0], loc.at[0]),
        pltpu.make_async_copy(q_hbm.at[0], q_own, loc.at[1]),
        pltpu.make_async_copy(k_hbm.at[0], kv_own.at[0], loc.at[2]),
        pltpu.make_async_copy(v_hbm.at[0], kv_own.at[1], loc.at[3]),
        pltpu.make_async_copy(g_hbm.at[0], g_in.at[z], loc.at[4]),
    ]
    for copy in local:
        copy.start()

    barrier = pltpu.get_barrier_semaphore()
    @pl.when(z > 0)
    def _():
        pl.semaphore_signal(barrier, inc=1, device_id={"sp": z - 1}, device_id_type=MESH)

    @pl.when(z < sp - 1)
    def _():
        pl.semaphore_signal(barrier, inc=1, device_id={"sp": z + 1}, device_id_type=MESH)

    for peer in (core, xs, ys):
        pl.semaphore_signal(barrier, inc=1, device_id={"dp": peer}, device_id_type=MESH)
    g_stage[...] = jnp.zeros_like(g_stage)
    pl.semaphore_wait(
        barrier, 3 + (z > 0).astype(jnp.int32) + (z < sp - 1).astype(jnp.int32)
    )

    for teller, pair in ((HUB + 1, (HUB, HUB + 2)), (HUB, (HUB - 1, HUB + 1))):
        @pl.when(z == teller)
        def _():
            for target in pair:
                pl.semaphore_signal(
                    seen_sem.at[teller - HUB], inc=1, device_id={"sp": target},
                    device_id_type=MESH,
                )

    def gate_copy(owner, target, relayed=0):
        return remote(g_in.at[owner], g_in.at[owner], g_ss.at[relayed], g_rs.at[0], sp=target)

    def q_copy(c, slot, target):
        return remote(
            q_own.at[:, cols(c)], q_in.at[slot, :, cols(c)], snd.at[0], in_rs.at[c], sp=target
        )

    def kv_copy(c):
        return remote(
            kv_own.at[:, :, cols(c)], kv_in.at[:, :, cols(c)], snd.at[0], in_rs.at[c], sp=HUB
        )

    whole = {1: 0, 3: 1, 5: 2, 7: 3}
    halves = {2: 4, 4: 6, 6: 8}

    def w_sem(slot, part):
        return w_rs.at[whole[slot] if slot in whole else halves[slot] + part]

    def w_copy(slot, part, bit, peer):
        span = pl.ds(part * half, half)
        return remote(
            w_buf.at[slot, span], w_buf.at[slot ^ bit, span], snd.at[1], w_sem(slot ^ bit, part), dp=peer
        )

    w_plan = {
        "first": [(0, 0, 2, xs), (0, 1, 4, ys), (0, 1, 2, xs), (0, 0, 4, ys), (0, 0, 1, core), (0, 1, 1, core)],
        "early": [(2, 0, 4, ys), (4, 1, 2, xs), (2, 0, 1, core), (4, 1, 1, core)],
        "middle": [(2, 1, 1, core), (4, 0, 1, core)],
        "late": [(6, 0, 1, core), (6, 1, 1, core)],
    }

    def w_arrived(slot, part=None):
        if part is None:
            arrived(w_buf.at[slot], w_sem(slot, 0))
        else:
            arrived(w_buf.at[slot, pl.ds(part * half, half)], w_sem(slot, part))

    def relay(stage):
        seen = []
        for slot, part, bit, peer in w_plan[stage]:
            if slot and (slot, part) not in seen:
                w_arrived(slot, part)
                seen.append((slot, part))
            w_copy(slot, part, bit, peer).start()

    local[0].wait()
    relay("first")
    for copy in local[1:]:
        copy.wait()

    for owner, target in ((0, 1), (1, 0), (1, 2), (2, 1), (2, 3), (3, 2)):
        @pl.when(z == owner)
        def _():
            gate_copy(owner, target).start()

    @pl.when(z == 0)
    def _():
        for c in range(chunks):
            kv_copy(c).start()
            if c == 0:
                pl.semaphore_wait(seen_sem.at[0], 1)
                gate_copy(0, 2).start()

    @pl.when(z == HUB + 1)
    def _():
        for c in range(chunks):
            q_copy(c, 0, HUB).start()
            if c == 0:
                pl.semaphore_wait(seen_sem.at[0], 1)
                gate_copy(2, 0).start()

    @pl.when(z == HUB + 2)
    def _():
        q_copy(0, 1, HUB + 1).start()
        pl.semaphore_wait(seen_sem.at[1], 1)
        gate_copy(3, 1).start()
        q_copy(0, 1, HUB).start()
        q_copy(1, 1, HUB).start()
        for c in range(1, chunks):
            q_copy(c, 1, HUB + 1).start()
            if c + 1 < chunks:
                q_copy(c + 1, 1, HUB).start()

    @pl.when(z == HUB)
    def _():
        pl.semaphore_wait(seen_sem.at[1], 1)
        gate_copy(1, 3).start()

    arrived(g_in.at[pl.ds(0, sp - 1)], g_rs.at[0])

    @pl.when(z == HUB)
    def _():
        gate_copy(0, 3, 1).start()
        gate_copy(3, 0, 1).start()

    per = g_in.shape[1]
    for c in range(chunks):
        for n in range(2):
            head = 2 * c + n
            g_row[c, n : n + 1, :] = g_in[head // per, head % per : head % per + 1, :]

    def key_gates(block):
        for owner in range(sp):
            rest = -g_in[owner, :, pl.ds(pl.multiple_of(block * rows, LANES), rows)]
            for n in range(3):
                piece = rest.astype(jnp.bfloat16).astype(jnp.float32)
                rest = rest - piece
                at = n * SPLIT + owner * per
                g_stage[at : at + per, :] = piece
        return g_stage[...].T.astype(g_key.dtype)

    g_key[1] = key_gates(z)

    @pl.when(z == HUB)
    def _():
        g_key[0] = key_gates(0)

    def work(c, qs, blocks, both, masks):
        k = kv_own[0, :, cols(c)]
        v = kv_own[1, :, cols(c)]
        gates = g_key[1]
        if both:
            k = jnp.concatenate([kv_in[0, :, cols(c)], k], axis=0)
            v = jnp.concatenate([kv_in[1, :, cols(c)], v], axis=0)
            gates = jnp.concatenate([g_key[0], gates], axis=0)
        row_gates = [
            g_row[c, :, pl.ds(pl.multiple_of(block * rows, LANES), rows)] for block in blocks
        ]
        return attend(
            c, [q[:, cols(c)] for q in qs], row_gates, k, v, gates, masks, scale, head_size
        )

    def finish(c, result):
        heads[:, cols(c)] = result.astype(heads.dtype).T

    def put(c, slot, result, lse):
        o_out[slot, c] = result.astype(o_out.dtype)
        s_out[slot, c] = lse

    def give(c, slot, into, target):
        remote(s_out.at[slot, c], s_in.at[into, c], snd.at[3], o_rs.at[c], sp=target).start()
        remote(o_out.at[slot, c], o_in.at[into, c], snd.at[2], o_rs.at[c], sp=target).start()

    @pl.when(z == 0)
    def _():
        @pl.loop(0, chunks // 2)
        def _(pair):
            for n in range(2):
                c = 2 * pair + n
                finish(c, work(c, [q_own], [z], False, [True])[0][0])

        relay("early")
        relay("middle")

    @pl.when(z == HUB)
    def _():
        @pl.loop(0, chunks)
        def _(c):
            @pl.when(c == chunks // 2)
            def _():
                relay("early")

            arrived(w_buf.at[0, pl.ds(0, 2 * rows)], in_rs.at[c])
            far, near, own = work(
                c, [q_in.at[1], q_in.at[0], q_own], [HUB + 2, HUB + 1, HUB], True, [False, False, True]
            )
            put(c, 1, *far)
            put(c, 0, *near)
            give(c, 1, 0, HUB + 2)
            give(c, 0, 0, HUB + 1)
            finish(c, own[0])

        relay("middle")

    @pl.when(z == HUB + 1)
    def _():
        @pl.loop(0, chunks)
        def _(c):
            @pl.when(c == chunks // 2)
            def _():
                relay("early")

            arrived(q_in.at[1, :, cols(c)], in_rs.at[c])
            far, own = work(c, [q_in.at[1], q_own], [HUB + 2, HUB + 1], False, [False, True])
            put(c, 1, *far)
            give(c, 1, 1, HUB + 2)
            o_own[c], s_own[c] = own

    @pl.when(z == HUB + 2)
    def _():
        @pl.loop(0, chunks // 2)
        def _(pair):
            for n in range(2):
                c = 2 * pair + n
                o_own[c], s_own[c] = work(c, [q_own], [z], False, [True])[0]

        relay("early")

    def merge(c, *pieces):
        top = functools.reduce(jnp.maximum, [lse for _, lse in pieces])
        scales = [jnp.exp(lse - top) for _, lse in pieces]
        total = 1.0 / functools.reduce(jnp.add, scales)
        scales = [scale * total for scale in scales]
        blocks = []
        for n in range(2):
            span = slice(n * head_size, (n + 1) * head_size)
            terms = [
                result[span].astype(jnp.float32) * scale[n : n + 1]
                for (result, _), scale in zip(pieces, scales)
            ]
            blocks.append(functools.reduce(jnp.add, terms))
        finish(c, jnp.concatenate(blocks, axis=0))

    @pl.when(z == HUB + 1)
    def _():
        @pl.loop(0, chunks)
        def _(c):
            @pl.when(c == chunks - 2)
            def _():
                relay("middle")

            arrived(one_part, o_rs.at[c])
            merge(c, (o_own[c], s_own[c]), (o_in[0, c], s_in[0, c]))

    @pl.when(z == HUB + 2)
    def _():
        @pl.loop(0, chunks)
        def _(c):
            @pl.when(c == chunks - 2)
            def _():
                relay("middle")

            arrived(two_parts, o_rs.at[c])
            merge(c, (o_own[c], s_own[c]), (o_in[0, c], s_in[0, c]), (o_in[1, c], s_in[1, c]))

    width = w_buf.shape[2]

    def project(slot):
        owner = d
        for bit in (1, 2, 4):
            if slot & bit:
                owner = flip(owner, bit)
        block = jnp.dot(heads[...], w_buf[slot], preferred_element_type=jnp.float32)
        out_ref[0, :, pl.ds(pl.multiple_of(owner * width, LANES), width)] = block.astype(
            out_ref.dtype
        )

    project(0)
    w_arrived(1)
    for slot in (1, 2, 4):
        project(slot)
    for slot in (3, 5):
        w_arrived(slot)
        project(slot)
    relay("late")
    project(6)
    w_arrived(7)
    project(7)

    sent(w_buf.at[pl.ds(0, 7)], snd.at[1])

    @pl.when((z == 0) | (z == HUB + 2))
    def _():
        sent(g_in.at[pl.ds(0, 2)], g_ss.at[0])
        sent(kv_own, snd.at[0])

    @pl.when((z == HUB) | (z == HUB + 1))
    def _():
        sent(g_in.at[pl.ds(0, 3)], g_ss.at[0])

    @pl.when(z == HUB)
    def _():
        sent(g_in.at[pl.ds(0, 2)], g_ss.at[1])
        sent(o_out, snd.at[2])
        sent(s_out, snd.at[3])

    @pl.when(z == HUB + 1)
    def _():
        sent(q_own, snd.at[0])
        sent(o_out.at[1], snd.at[2])
        sent(s_out.at[1], snd.at[3])


def fused_shards(sp, queries, keys, values, cum_gates, out_weight):
    _, rows, width = queries.shape
    _, per, length = cum_gates.shape
    head_size = width // (per * sp)
    depth, block = out_weight.shape
    dp = 8
    chunks = width // LANES
    bf16, f32 = queries.dtype, jnp.float32
    dma = pltpu.SemaphoreType.DMA
    return pl.pallas_call(
        functools.partial(layer_kernel, (sp, chunks, head_size, head_size ** (-0.5))),
        out_shape=jax.ShapeDtypeStruct((1, rows, block * dp), bf16),
        in_specs=[pl.BlockSpec(memory_space=pltpu.HBM)] * 5,
        out_specs=pl.BlockSpec(memory_space=pltpu.VMEM),
        scratch_shapes=[
            pltpu.VMEM((rows, width), bf16),
            pltpu.VMEM((2, rows, width), bf16),
            pltpu.VMEM((2, rows, width), bf16),
            pltpu.VMEM((2, rows, width), bf16),
            pltpu.VMEM((sp, per, length), f32),
            pltpu.VMEM((chunks, 2, length), f32),
            pltpu.VMEM((LANES, rows), f32),
            pltpu.VMEM((2, rows, LANES), bf16),
            pltpu.VMEM((2, chunks, LANES, rows), bf16),
            pltpu.VMEM((2, chunks, 2, rows), f32),
            pltpu.VMEM((2, chunks, LANES, rows), bf16),
            pltpu.VMEM((2, chunks, 2, rows), f32),
            pltpu.VMEM((chunks, LANES, rows), f32),
            pltpu.VMEM((chunks, 2, rows), f32),
            pltpu.VMEM((rows, width), bf16),
            pltpu.VMEM((dp, depth, block), bf16),
            pltpu.VMEM((LANES // 4 + 1, 2, rows), f32),
            pltpu.VMEM((LANES // 2 + 2, 2, rows), f32),
            dma((chunks,)), dma((chunks,)), dma((4,)), dma((1,)), dma((2,)), dma((10,)), dma((5,)),
            pltpu.SemaphoreType.REGULAR((2,)),
        ],
        compiler_params=pltpu.CompilerParams(collective_id=0, has_side_effects=True, vmem_limit_bytes=16 * 2**20),
        name="layer",
    )(*(pltpu.with_memory_space_constraint(x, pltpu.HBM) for x in (queries, keys, values, cum_gates, out_weight)))


def route(sp, dp, queries, keys, values, cum_gates, out_weight):
    _, rows, width = queries.shape
    head_size = width // (cum_gates.shape[1] * sp)
    fits = (
        sp == HUB + 3
        and dp == 8
        and rows == LANES
        and 2 * head_size == LANES
        and width % (2 * LANES) == 0
        and cum_gates.shape[1] * sp <= SPLIT
        and out_weight.shape[1] % (2 * LANES) == 0
    )
    if fits:
        return fused_shards(sp, queries, keys, values, cum_gates, out_weight)
    return shards(queries, keys, values, cum_gates, out_weight)


def solution(mesh):
    in_specs = (
        P("dp", "sp", None),
        P("dp", "sp", None),
        P("dp", "sp", None),
        P("dp", "sp", None),
        P(None, "dp"),
    )
    out_specs = P("dp", "sp", None)
    body = functools.partial(route, mesh.shape["sp"], mesh.shape["dp"])
    return jax.shard_map(body, mesh=mesh, in_specs=in_specs, out_specs=out_specs, check_vma=False)
```

time: 28.4 us -> 24.8 us (0.87)
  Pallas kernels: 27.4 us -> 23.5 us
    pallas_call x1, Pallas kernels: 27.4 us -> 23.5 us  [fused_shards(): pl.pallas_call(functools.partial(layer_kernel, (sp, chunks, head_size, he...]
where the time goes in v1:
time: 24.8 us; the launch traced here: 24.3 us
  Pallas kernels  23.5 us (95%)
  local copies, waits for them, and re-layouts  0.8 us (3%)
    pallas_call x1, Pallas kernels, fused_shards(): pl.pallas_call(functools.partial(layer_kernel, (sp, chunks, head_size, he...  23.5 us
    unnamed x1, local copies, waits for them, and re-layouts  0.8 us

profile of v1, /device:TPU:19, one launch (start us, length us, event | category | flops | bytes accessed | tf_op | source)
XLA Modules:
  0.0 24.3 jit_solution(17721371647087478720)
XLA Ops:
  0.0 23.5 %layer.1 = bf16[1,128,2048]{2,1,0:T(8,128)(2,1)S(1)} custom-call(bf16[1,128,1024]{2,1,0:T(8,128)(2,1)} %q_hbm.1, bf16[1,128,1024]{2,1,0:T(8,128)(2,1)} %k_hbm.1, bf16[1,128,1024]{2,1,0:T(8,128)(2,1)} %v_hbm.1, f32[1,4,512]{2,1,0:T(4,128)} %g_hbm.1, bf16[1024,256]{1,0:T(8,128)(2,1)} %w_hbm.1), custom_call_target="tpu_custom_call" | custom-call | tf_op jit(solution)/shard_map/layer/pallas_call | solution.py:474
  23.5 0.8 %copy.7 = bf16[1,128,2048]{2,1,0:T(8,128)(2,1)} copy(bf16[1,128,2048]{2,1,0:T(8,128)(2,1)S(1)} %layer.1) | data formatting | bytes 1048576

commit v2 on v1

--- a/solution.py
+++ b/solution.py
@@ -64,6 +64,7 @@
 LANES = 128
 HUB = 1
 SPLIT = 32
+EARLY = (0, 1, 2, 4)
 
 
 def flip(index, bit):
@@ -119,7 +120,7 @@
 def layer_kernel(
     sizes, q_hbm, k_hbm, v_hbm, g_hbm, w_hbm, out_ref,
     q_own, q_in, kv_own, kv_in, g_in, g_row, g_stage, g_key, o_out, s_out, o_in, s_in, o_own, s_own,
-    heads, w_buf, one_part, two_parts,
+    o_far, s_far, total, heads, w_buf, one_part, two_parts,
     in_rs, o_rs, snd, g_rs, g_ss, w_rs, loc, seen_sem,
 ):
     sp, chunks, head_size, scale = sizes
@@ -179,11 +180,16 @@
                 )
 
     def gate_copy(owner, target, relayed=0):
-        return remote(g_in.at[owner], g_in.at[owner], g_ss.at[relayed], g_rs.at[0], sp=target)
+        late = owner == HUB + 2 and target == HUB
+        return remote(
+            g_in.at[owner], g_in.at[owner], g_ss.at[relayed], g_rs.at[1 if late else 0], sp=target
+        )
 
     def q_copy(c, slot, target):
+        lone = slot == 1 and target == HUB and c == 0
         return remote(
-            q_own.at[:, cols(c)], q_in.at[slot, :, cols(c)], snd.at[0], in_rs.at[c], sp=target
+            q_own.at[:, cols(c)], q_in.at[slot, :, cols(c)], snd.at[0],
+            in_rs.at[chunks if lone else c], sp=target,
         )
 
     def kv_copy(c):
@@ -191,41 +197,145 @@
             kv_own.at[:, :, cols(c)], kv_in.at[:, :, cols(c)], snd.at[0], in_rs.at[c], sp=HUB
         )
 
-    whole = {1: 0, 3: 1, 5: 2, 7: 3}
-    halves = {2: 4, 4: 6, 6: 8}
-
-    def w_sem(slot, part):
-        return w_rs.at[whole[slot] if slot in whole else halves[slot] + part]
-
-    def w_copy(slot, part, bit, peer):
-        span = pl.ds(part * half, half)
-        return remote(
-            w_buf.at[slot, span], w_buf.at[slot ^ bit, span], snd.at[1], w_sem(slot ^ bit, part), dp=peer
-        )
-
-    w_plan = {
-        "first": [(0, 0, 2, xs), (0, 1, 4, ys), (0, 1, 2, xs), (0, 0, 4, ys), (0, 0, 1, core), (0, 1, 1, core)],
-        "early": [(2, 0, 4, ys), (4, 1, 2, xs), (2, 0, 1, core), (4, 1, 1, core)],
-        "middle": [(2, 1, 1, core), (4, 0, 1, core)],
-        "late": [(6, 0, 1, core), (6, 1, 1, core)],
-    }
-
-    def w_arrived(slot, part=None):
-        if part is None:
-            arrived(w_buf.at[slot], w_sem(slot, 0))
-        else:
-            arrived(w_buf.at[slot, pl.ds(part * half, half)], w_sem(slot, part))
-
-    def relay(stage):
-        seen = []
-        for slot, part, bit, peer in w_plan[stage]:
-            if slot and (slot, part) not in seen:
-                w_arrived(slot, part)
-                seen.append((slot, part))
-            w_copy(slot, part, bit, peer).start()
+    depth = w_buf.shape[1]
+    shed = depth // 8
+    odd = z % 2
+    parts = {}
+    for slot, front, back in ((2, 0, half), (4, half, 0)):
+        parts[slot, "first"] = (front, half // 2)
+        parts[slot, "second"] = (front + half // 2, half // 2)
+        parts[slot, "lent"] = (back + 2 * shed * (1 - odd), 2 * shed)
+        parts[slot, "rest"] = (back + shed * (1 + odd), shed)
+        parts[slot, "given"] = (back + 3 * shed * odd, shed)
+        parts[slot, "swap"] = (back + 3 * shed * (1 - odd), shed)
+        parts[slot, "wide"] = (back, 2 * shed)
+        parts[slot, "some"] = (back + 5 * shed // 2, 3 * shed // 2)
+        parts[slot, "bit"] = (back + 2 * shed, shed // 2)
+    alias = {"wide": "given", "some": "given", "bit": "rest"}
+    names = ["first", "second", "rest", "lent", "given"]
+
+    for slot in (2, 4):
+        start, size = parts[slot, "second"]
+        parts[slot, "kept"] = (start, size // 2)
+        parts[slot, "moved"] = (start + size // 2, size // 2)
+    lasts = ["first", "kept", "moved"]
+
+    def w_sem(slot, name):
+        if name is None:
+            return w_rs.at[slot // 2]
+        if slot in (2, 4):
+            return w_rs.at[4 + 5 * (slot == 4) + names.index(name)]
+        base = {6: 14, 7: 20, 3: 22, 5: 23}[slot]
+        if slot == 6:
+            base += lasts.index(name[0]) + 3 * (name[1] == 4)
+        if slot == 7:
+            base += name[1] == 4
+        return w_rs.at[base]
+
+    def w_ref(slot, rows_of):
+        start, size = rows_of
+        return w_buf.at[slot, pl.ds(pl.multiple_of(start, 16), size)]
+
+    def w_copy(slot, into, rows_of, ss, rs, **device):
+        remote(w_ref(slot, rows_of), w_ref(into, rows_of), snd.at[ss], rs, **device).start()
+
+    def w_first():
+        def spread(name):
+            w_copy(0, 2, parts[2, name], 4, w_sem(2, alias.get(name, name)), dp=xs)
+            w_copy(0, 4, parts[4, name], 4, w_sem(4, alias.get(name, name)), dp=ys)
+
+        spread("lent")
+        w_copy(0, 1, (0, depth), 1, w_sem(1, None), dp=core)
+        spread("first")
+        spread("second")
+
+        @pl.when(z > HUB)
+        def _():
+            spread("rest")
+
+        @pl.when(z == HUB)
+        def _():
+            spread("bit")
+
+    turns = {2: (4, ys), 4: (2, xs)}
+
+    def w_got(name):
+        for slot in (2, 4):
+            piece = parts[slot, name]
+            arrived(w_ref(slot, piece), w_sem(slot, alias.get(name, name)))
+            peer = turns[slot][1]
+            if name == "first":
+                w_copy(slot, 6, piece, 4, w_sem(6, ("first", slot)), dp=peer)
+            if name == "second":
+                w_copy(slot, 6, parts[slot, "kept"], 4, w_sem(6, ("kept", slot)), dp=peer)
+
+                @pl.when(d % 2 == 1)
+                def _():
+                    w_copy(slot, 6, parts[slot, "moved"], 4, w_sem(6, ("moved", slot)), dp=peer)
+
+            into = w_sem(slot + 1, "second" if name == "second" else None)
+            w_copy(slot, slot + 1, piece, 1, into, dp=core)
+
+    def w_cross():
+        @pl.when(d % 2 == 1)
+        def _():
+            for slot in (2, 4):
+                arrived(w_ref(slot + 1, parts[slot, "second"]), w_sem(slot + 1, "second"))
+                w_copy(slot + 1, 7, parts[slot, "moved"], 4, w_sem(7, ("moved", slot)), dp=turns[slot][1])
+
+    def w_lend():
+        for giver, sends in (
+            (0, [(2, "some", 1)]),
+            (1, [(2, "lent", 0), (4, "lent", 0)]),
+            (2, [(2, "swap", 3), (4, "swap", 3), (4, "some", 1)]),
+            (3, [(2, "swap", 2), (4, "swap", 2)]),
+        ):
+            @pl.when(z == giver)
+            def _():
+                for slot, name, target in sends:
+                    w_copy(slot, slot, parts[slot, name], 5, w_sem(slot, "given"), sp=target)
+
+    def w_diag(name):
+        for slot in (2, 4):
+            for part in ("first",) if name == "first" else ("kept",):
+                arrived(w_ref(6, parts[slot, part]), w_sem(6, (part, slot)))
+                w_copy(6, 7, parts[slot, part], 1, w_sem(7, None), dp=core)
+        if name == "second":
+            @pl.when(d % 2 == 1)
+            def _():
+                for slot in (2, 4):
+                    piece = parts[slot, "moved"]
+                    arrived(w_ref(6, piece), w_sem(6, ("moved", slot)))
+                    w_copy(6, 7, piece, 1, w_sem(7, None), dp=core)
+                for slot in (2, 4):
+                    piece = parts[slot, "moved"]
+                    arrived(w_ref(7, piece), w_sem(7, ("moved", slot)))
+                    w_copy(7, 6, piece, 1, w_sem(6, ("moved", slot)), dp=core)
+
+    def w_arrived(slot):
+        if slot == 1:
+            arrived(w_buf.at[slot], w_sem(slot, None))
+            return
+        short = w_buf.at[slot, pl.ds(0, depth - 2 * shed)]
+        if slot == 7:
+            @pl.when(d % 2 == 0)
+            def _():
+                arrived(w_buf.at[slot], w_sem(slot, None))
+                for near in (2, 4):
+                    arrived(w_ref(6, parts[near, "moved"]), w_sem(6, ("moved", near)))
+
+            @pl.when(d % 2 == 1)
+            def _():
+                arrived(short, w_sem(slot, None))
+            return
+        arrived(short, w_sem(slot, None))
+
+        @pl.when(d % 2 == 0)
+        def _():
+            arrived(w_ref(slot, parts[slot - 1, "second"]), w_sem(slot, "second"))
 
     local[0].wait()
-    relay("first")
+    w_first()
     for copy in local[1:]:
         copy.wait()
 
@@ -267,21 +377,33 @@
         pl.semaphore_wait(seen_sem.at[1], 1)
         gate_copy(1, 3).start()
 
-    arrived(g_in.at[pl.ds(0, sp - 1)], g_rs.at[0])
+    @pl.when(z != HUB)
+    def _():
+        w_got("lent")
+        w_lend()
+
+    @pl.when(z == 0)
+    def _():
+        w_got("first")
 
     @pl.when(z == HUB)
     def _():
-        gate_copy(0, 3, 1).start()
-        gate_copy(3, 0, 1).start()
+        arrived(g_in.at[pl.ds(0, sp - 2)], g_rs.at[0])
+
+    @pl.when(z != HUB)
+    def _():
+        arrived(g_in.at[pl.ds(0, sp - 1)], g_rs.at[0])
 
     per = g_in.shape[1]
-    for c in range(chunks):
-        for n in range(2):
-            head = 2 * c + n
-            g_row[c, n : n + 1, :] = g_in[head // per, head % per : head % per + 1, :]
-
-    def key_gates(block):
-        for owner in range(sp):
+
+    def row_gates(owners):
+        for owner in owners:
+            for at in range(per):
+                c, n = divmod(owner * per + at, 2)
+                g_row[c, n : n + 1, :] = g_in[owner, at : at + 1, :]
+
+    def key_gates(block, owners):
+        for owner in owners:
             rest = -g_in[owner, :, pl.ds(pl.multiple_of(block * rows, LANES), rows)]
             for n in range(3):
                 piece = rest.astype(jnp.bfloat16).astype(jnp.float32)
@@ -290,11 +412,19 @@
                 g_stage[at : at + per, :] = piece
         return g_stage[...].T.astype(g_key.dtype)
 
-    g_key[1] = key_gates(z)
+    def hub_gates(owners):
+        row_gates(owners)
+        for n in range(2):
+            g_key[n] = key_gates(n + HUB - 1, range(owners[-1] + 1))
 
     @pl.when(z == HUB)
     def _():
-        g_key[0] = key_gates(0)
+        hub_gates(range(HUB + 2))
+
+    @pl.when(z != HUB)
+    def _():
+        row_gates(range(sp))
+        g_key[1] = key_gates(z, range(sp))
 
     def work(c, qs, blocks, both, masks):
         k = kv_own[0, :, cols(c)]
@@ -304,11 +434,11 @@
             k = jnp.concatenate([kv_in[0, :, cols(c)], k], axis=0)
             v = jnp.concatenate([kv_in[1, :, cols(c)], v], axis=0)
             gates = jnp.concatenate([g_key[0], gates], axis=0)
-        row_gates = [
+        rows_of = [
             g_row[c, :, pl.ds(pl.multiple_of(block * rows, LANES), rows)] for block in blocks
         ]
         return attend(
-            c, [q[:, cols(c)] for q in qs], row_gates, k, v, gates, masks, scale, head_size
+            c, [q[:, cols(c)] for q in qs], rows_of, k, v, gates, masks, scale, head_size
         )
 
     def finish(c, result):
@@ -322,62 +452,7 @@
         remote(s_out.at[slot, c], s_in.at[into, c], snd.at[3], o_rs.at[c], sp=target).start()
         remote(o_out.at[slot, c], o_in.at[into, c], snd.at[2], o_rs.at[c], sp=target).start()
 
-    @pl.when(z == 0)
-    def _():
-        @pl.loop(0, chunks // 2)
-        def _(pair):
-            for n in range(2):
-                c = 2 * pair + n
-                finish(c, work(c, [q_own], [z], False, [True])[0][0])
-
-        relay("early")
-        relay("middle")
-
-    @pl.when(z == HUB)
-    def _():
-        @pl.loop(0, chunks)
-        def _(c):
-            @pl.when(c == chunks // 2)
-            def _():
-                relay("early")
-
-            arrived(w_buf.at[0, pl.ds(0, 2 * rows)], in_rs.at[c])
-            far, near, own = work(
-                c, [q_in.at[1], q_in.at[0], q_own], [HUB + 2, HUB + 1, HUB], True, [False, False, True]
-            )
-            put(c, 1, *far)
-            put(c, 0, *near)
-            give(c, 1, 0, HUB + 2)
-            give(c, 0, 0, HUB + 1)
-            finish(c, own[0])
-
-        relay("middle")
-
-    @pl.when(z == HUB + 1)
-    def _():
-        @pl.loop(0, chunks)
-        def _(c):
-            @pl.when(c == chunks // 2)
-            def _():
-                relay("early")
-
-            arrived(q_in.at[1, :, cols(c)], in_rs.at[c])
-            far, own = work(c, [q_in.at[1], q_own], [HUB + 2, HUB + 1], False, [False, True])
-            put(c, 1, *far)
-            give(c, 1, 1, HUB + 2)
-            o_own[c], s_own[c] = own
-
-    @pl.when(z == HUB + 2)
-    def _():
-        @pl.loop(0, chunks // 2)
-        def _(pair):
-            for n in range(2):
-                c = 2 * pair + n
-                o_own[c], s_own[c] = work(c, [q_own], [z], False, [True])[0]
-
-        relay("early")
-
-    def merge(c, *pieces):
+    def merge(*pieces):
         top = functools.reduce(jnp.maximum, [lse for _, lse in pieces])
         scales = [jnp.exp(lse - top) for _, lse in pieces]
         total = 1.0 / functools.reduce(jnp.add, scales)
@@ -390,55 +465,249 @@
                 for (result, _), scale in zip(pieces, scales)
             ]
             blocks.append(functools.reduce(jnp.add, terms))
-        finish(c, jnp.concatenate(blocks, axis=0))
-
-    @pl.when(z == HUB + 1)
-    def _():
-        @pl.loop(0, chunks)
-        def _(c):
-            @pl.when(c == chunks - 2)
-            def _():
-                relay("middle")
-
-            arrived(one_part, o_rs.at[c])
-            merge(c, (o_own[c], s_own[c]), (o_in[0, c], s_in[0, c]))
-
-    @pl.when(z == HUB + 2)
-    def _():
-        @pl.loop(0, chunks)
-        def _(c):
-            @pl.when(c == chunks - 2)
-            def _():
-                relay("middle")
-
-            arrived(two_parts, o_rs.at[c])
-            merge(c, (o_own[c], s_own[c]), (o_in[0, c], s_in[0, c]), (o_in[1, c], s_in[1, c]))
-
+        return jnp.concatenate(blocks, axis=0), top - jnp.log(total)
+
+    def on(c, step, run, *args):
+        @pl.when(c == step)
+        def _():
+            run(*args)
+
+    cut = chunks // 2
     width = w_buf.shape[2]
 
-    def project(slot):
+    def product(slot, start, stop):
+        span = pl.ds(start * LANES, (stop - start) * LANES)
+        return jnp.dot(heads[:, span], w_buf[slot, span], preferred_element_type=jnp.float32)
+
+    def store(slot, block):
         owner = d
         for bit in (1, 2, 4):
             if slot & bit:
                 owner = flip(owner, bit)
-        block = jnp.dot(heads[...], w_buf[slot], preferred_element_type=jnp.float32)
         out_ref[0, :, pl.ds(pl.multiple_of(owner * width, LANES), width)] = block.astype(
             out_ref.dtype
         )
 
-    project(0)
-    w_arrived(1)
-    for slot in (1, 2, 4):
-        project(slot)
-    for slot in (3, 5):
-        w_arrived(slot)
-        project(slot)
-    relay("late")
-    project(6)
-    w_arrived(7)
-    project(7)
-
-    sent(w_buf.at[pl.ds(0, 7)], snd.at[1])
+    def project(slot):
+        store(slot, product(slot, 0, chunks))
+
+    def remain(start):
+        for n, slot in enumerate(EARLY):
+            store(slot, total[n] + product(slot, start, chunks))
+
+    def gather(stop):
+        w_arrived(1)
+        for n, slot in enumerate(EARLY):
+            if stop == chunks:
+                project(slot)
+            else:
+                total[n] = product(slot, 0, stop)
+
+    def ends(stop):
+        @pl.when(d % 2 == 0)
+        def _():
+            w_diag("second")
+
+        gather(stop)
+
+        @pl.when(d % 2 == 1)
+        def _():
+            w_diag("second")
+
+    @pl.when(z == 0)
+    def _():
+        @pl.loop(0, chunks // 2)
+        def _(pair):
+            for n in range(2):
+                c = 2 * pair + n
+                finish(c, work(c, [q_own], [z], False, [True])[0][0])
+
+        w_got("second")
+        w_got("wide")
+        w_cross()
+        gather(chunks)
+        w_diag("first")
+        w_diag("second")
+
+    @pl.when(z == HUB)
+    def _():
+        def hub(c, joined):
+            arrived(w_buf.at[0, pl.ds(0, 2 * rows)], in_rs.at[c])
+            far, near, own = work(
+                c, [q_in.at[1], q_in.at[0], q_own], [HUB + 2, HUB + 1, HUB], True, [False, False, True]
+            )
+            put(c, 1, *far)
+            put(c, 0, *near)
+            if joined:
+                give(c, 1, 1, HUB + 1)
+            else:
+                give(c, 1, 0, HUB + 2)
+            give(c, 0, 0, HUB + 1)
+            finish(c, own[0])
+
+        arrived(w_buf.at[0, pl.ds(0, 3 * rows // 2)], in_rs.at[0])
+        near, own = work(0, [q_in.at[0], q_own], [HUB + 1, HUB], True, [False, True])
+        put(0, 0, *near)
+        give(0, 0, 0, HUB + 1)
+        finish(0, own[0])
+        arrived(g_in.at[0], g_rs.at[1])
+        gate_copy(0, 3, 1).start()
+        gate_copy(3, 0, 1).start()
+        hub_gates(range(HUB + 2, sp))
+        arrived(w_buf.at[0, pl.ds(0, rows // 2)], in_rs.at[chunks])
+        put(0, 1, *work(0, [q_in.at[1]], [HUB + 2], True, [False])[0])
+        give(0, 1, 0, HUB + 2)
+        w_got("lent")
+        w_lend()
+
+        @pl.loop(1, cut + 1)
+        def _(c):
+            on(c, 3, w_got, "first")
+            hub(c, True)
+
+        w_got("second")
+
+        @pl.loop(cut + 1, chunks)
+        def _(c):
+            @pl.when(c == chunks - 1)
+            def _():
+                w_got("bit")
+                w_cross()
+                w_diag("first")
+
+            hub(c, False)
+
+        w_got("some")
+        ends(chunks)
+
+    @pl.when(z == HUB + 1)
+    def _():
+        def near(c, joined):
+            arrived(q_in.at[1, :, cols(c)], in_rs.at[c])
+            far, own = work(c, [q_in.at[1], q_own], [HUB + 2, HUB + 1], False, [False, True])
+            if joined:
+                o_far[c - 1], s_far[c - 1] = far
+            else:
+                put(c, 1, *far)
+                give(c, 1, 1, HUB + 2)
+            o_own[c], s_own[c] = own
+
+        def join(c, joined):
+            arrived(two_parts if joined else one_part, o_rs.at[c])
+            if joined:
+                put(c, 1, *merge((o_far[c - 1], s_far[c - 1]), (o_in[1, c], s_in[1, c])))
+                give(c, 1, 1, HUB + 2)
+            finish(c, merge((o_own[c], s_own[c]), (o_in[0, c], s_in[0, c]))[0])
+
+        near(0, False)
+
+        @pl.loop(1, cut + 1)
+        def _(c):
+            on(c, 3, w_got, "first")
+            near(c, True)
+
+        join(0, False)
+        join(1, True)
+
+        @pl.loop(cut + 1, chunks)
+        def _(c):
+            on(c, cut + 1, w_got, "second")
+
+            @pl.when(c == chunks - 1)
+            def _():
+                w_got("rest")
+                w_cross()
+
+            near(c, False)
+            join(c - cut + 1, True)
+
+        w_diag("first")
+        w_got("given")
+
+        @pl.loop(cut + 1, chunks - 1)
+        def _(c):
+            join(c, False)
+
+        ends(chunks - 1)
+        join(chunks - 1, False)
+        remain(chunks - 1)
+
+    @pl.when(z == HUB + 2)
+    def _():
+        @pl.loop(0, chunks // 2)
+        def _(pair):
+            for n in range(2):
+                c = 2 * pair + n
+                o_own[c], s_own[c] = work(c, [q_own], [z], False, [True])[0]
+
+        def join(c, joined):
+            arrived(one_part if joined else two_parts, o_rs.at[c])
+            pieces = [(o_own[c], s_own[c]), (o_in[1, c], s_in[1, c])]
+            if not joined:
+                pieces.append((o_in[0, c], s_in[0, c]))
+            finish(c, merge(*pieces)[0])
+
+        w_got("first")
+        w_got("second")
+        w_got("rest")
+        w_cross()
+        w_diag("first")
+        w_got("given")
+        join(0, False)
+
+        @pl.loop(1, cut - 1)
+        def _(c):
+            join(c, True)
+
+        @pl.when(d % 2 == 0)
+        def _():
+            w_diag("second")
+
+        join(cut - 1, True)
+        gather(cut)
+
+        @pl.when(d % 2 == 1)
+        def _():
+            w_diag("second")
+
+        join(cut, True)
+
+        @pl.loop(cut + 1, chunks)
+        def _(c):
+            join(c, False)
+
+        w_arrived(3)
+        w_arrived(5)
+        w_arrived(7)
+        remain(cut)
+        for slot in (3, 5, 6, 7):
+            project(slot)
+
+    @pl.when(z <= HUB + 1)
+    def _():
+        for slot in (3, 5):
+            w_arrived(slot)
+        for slot in (3, 5):
+            project(slot)
+        w_arrived(7)
+        for slot in (6, 7):
+            project(slot)
+
+    for parity in range(2):
+        @pl.when(d % 2 == parity)
+        def _():
+            moved = (2 * parity - 1) * shed
+            sent(w_buf.at[:, pl.ds(0, depth // 2 + moved // 4)], snd.at[1])
+            for plane in range(sp):
+                @pl.when(z == plane)
+                def _():
+                    each = 5 * depth // 8 + (0, shed // 4, shed // 2, shed // 2)[plane] + moved // 2
+                    sent(w_buf.at[pl.ds(0, 4), pl.ds(0, each)], snd.at[4])
+
+    for giver, count in enumerate((3, 8, 7, 4)):
+        @pl.when(z == giver)
+        def _():
+            sent(w_buf.at[0, pl.ds(0, count * shed // 2)], snd.at[5])
 
     @pl.when((z == 0) | (z == HUB + 2))
     def _():
@@ -491,11 +760,14 @@
             pltpu.VMEM((2, chunks, 2, rows), f32),
             pltpu.VMEM((chunks, LANES, rows), f32),
             pltpu.VMEM((chunks, 2, rows), f32),
+            pltpu.VMEM((chunks // 2, LANES, rows), f32),
+            pltpu.VMEM((chunks // 2, 2, rows), f32),
+            pltpu.VMEM((len(EARLY), rows, block), f32),
             pltpu.VMEM((rows, width), bf16),
             pltpu.VMEM((dp, depth, block), bf16),
             pltpu.VMEM((LANES // 4 + 1, 2, rows), f32),
             pltpu.VMEM((LANES // 2 + 2, 2, rows), f32),
-            dma((chunks,)), dma((chunks,)), dma((4,)), dma((1,)), dma((2,)), dma((10,)), dma((5,)),
+            dma((chunks + 1,)), dma((chunks,)), dma((6,)), dma((2,)), dma((2,)), dma((24,)), dma((5,)),
             pltpu.SemaphoreType.REGULAR((2,)),
         ],
         compiler_params=pltpu.CompilerParams(collective_id=0, has_side_effects=True, vmem_limit_bytes=16 * 2**20),
@@ -511,7 +783,8 @@
         and dp == 8
         and rows == LANES
         and 2 * head_size == LANES
-        and width % (2 * LANES) == 0
+        and width == 8 * LANES
+        and out_weight.shape[0] % (2 * LANES) == 0
         and cum_gates.shape[1] * sp <= SPLIT
         and out_weight.shape[1] % (2 * LANES) == 0
     )

time: 24.8 us -> 22.7 us (0.915)
  Pallas kernels: 23.5 us -> 21.6 us
    pallas_call x1, Pallas kernels: 23.5 us -> 21.6 us  [fused_shards(): pl.pallas_call(functools.partial(layer_kernel, (sp, chunks, head_size, he...]
where the time goes in v2:
time: 22.7 us; the launch traced here: 22.4 us
  Pallas kernels  21.6 us (95%)
  local copies, waits for them, and re-layouts  0.8 us (4%)
    pallas_call x1, Pallas kernels, fused_shards(): pl.pallas_call(functools.partial(layer_kernel, (sp, chunks, head_size, he...  21.6 us
    unnamed x1, local copies, waits for them, and re-layouts  0.8 us

profile of v2, /device:TPU:19, one launch (start us, length us, event | category | flops | bytes accessed | tf_op | source)
XLA Modules:
  0.0 22.4 jit_solution(7335928540892106101)
XLA Ops:
  0.0 21.6 %layer.1 = bf16[1,128,2048]{2,1,0:T(8,128)(2,1)S(1)} custom-call(bf16[1,128,1024]{2,1,0:T(8,128)(2,1)} %q_hbm.1, bf16[1,128,1024]{2,1,0:T(8,128)(2,1)} %k_hbm.1, bf16[1,128,1024]{2,1,0:T(8,128)(2,1)} %v_hbm.1, f32[1,4,512]{2,1,0:T(4,128)} %g_hbm.1, bf16[1024,256]{1,0:T(8,128)(2,1)} %w_hbm.1), custom_call_target="tpu_custom_call" | custom-call | tf_op jit(solution)/shard_map/layer/pallas_call | solution.py:743
  21.6 0.8 %copy.7 = bf16[1,128,2048]{2,1,0:T(8,128)(2,1)} copy(bf16[1,128,2048]{2,1,0:T(8,128)(2,1)S(1)} %layer.1) | data formatting | bytes 1048576

commit v3 on v2

--- a/solution.py
+++ b/solution.py
@@ -65,6 +65,8 @@
 HUB = 1
 SPLIT = 32
 EARLY = (0, 1, 2, 4)
+JOINED = (2, 5)
+THIN = 4
 
 
 def flip(index, bit):
@@ -147,9 +149,9 @@
     local = [
         pltpu.make_async_copy(w_hbm, w_buf.at[0], loc.at[0]),
         pltpu.make_async_copy(q_hbm.at[0], q_own, loc.at[1]),
-        pltpu.make_async_copy(k_hbm.at[0], kv_own.at[0], loc.at[2]),
+        pltpu.make_async_copy(g_hbm.at[0], g_in.at[z], loc.at[2]),
+        pltpu.make_async_copy(k_hbm.at[0], kv_own.at[0], loc.at[3]),
         pltpu.make_async_copy(v_hbm.at[0], kv_own.at[1], loc.at[3]),
-        pltpu.make_async_copy(g_hbm.at[0], g_in.at[z], loc.at[4]),
     ]
     for copy in local:
         copy.start()
@@ -175,7 +177,7 @@
         def _():
             for target in pair:
                 pl.semaphore_signal(
-                    seen_sem.at[teller - HUB], inc=1, device_id={"sp": target},
+                    seen_sem, inc=1, device_id={"sp": target},
                     device_id_type=MESH,
                 )
 
@@ -211,7 +213,10 @@
         parts[slot, "wide"] = (back, 2 * shed)
         parts[slot, "some"] = (back + 5 * shed // 2, 3 * shed // 2)
         parts[slot, "bit"] = (back + 2 * shed, shed // 2)
-    alias = {"wide": "given", "some": "given", "bit": "rest"}
+        thin = THIN * shed // 4
+        parts[slot, "thin"] = (back + 4 * shed - thin, thin)
+        parts[slot, "most"] = (back + 2 * shed, 2 * shed - thin)
+    alias = {"wide": "given", "some": "given", "bit": "rest", "thin": "given", "most": "rest"}
     names = ["first", "second", "rest", "lent", "given"]
 
     for slot in (2, 4):
@@ -222,15 +227,15 @@
 
     def w_sem(slot, name):
         if name is None:
-            return w_rs.at[slot // 2]
+            return w_rs.at[slot // 3]
         if slot in (2, 4):
-            return w_rs.at[4 + 5 * (slot == 4) + names.index(name)]
-        base = {6: 14, 7: 20, 3: 22, 5: 23}[slot]
+            return w_rs.at[3 + names.index(name)]
         if slot == 6:
-            base += lasts.index(name[0]) + 3 * (name[1] == 4)
-        if slot == 7:
-            base += name[1] == 4
-        return w_rs.at[base]
+            return w_rs.at[8 + lasts.index(name)]
+        return w_rs.at[11 + (slot != 7)]
+
+    def w_both(slot, name, size):
+        arrived(w_buf.at[0, pl.ds(0, 2 * size)], w_sem(slot, name))
 
     def w_ref(slot, rows_of):
         start, size = rows_of
@@ -249,10 +254,14 @@
         spread("first")
         spread("second")
 
-        @pl.when(z > HUB)
+        @pl.when(z == HUB + 1)
         def _():
             spread("rest")
 
+        @pl.when(z == HUB + 2)
+        def _():
+            spread("most")
+
         @pl.when(z == HUB)
         def _():
             spread("bit")
@@ -260,18 +269,18 @@
     turns = {2: (4, ys), 4: (2, xs)}
 
     def w_got(name):
+        w_both(2, alias.get(name, name), parts[2, name][1])
         for slot in (2, 4):
             piece = parts[slot, name]
-            arrived(w_ref(slot, piece), w_sem(slot, alias.get(name, name)))
             peer = turns[slot][1]
             if name == "first":
-                w_copy(slot, 6, piece, 4, w_sem(6, ("first", slot)), dp=peer)
+                w_copy(slot, 6, piece, 4, w_sem(6, "first"), dp=peer)
             if name == "second":
-                w_copy(slot, 6, parts[slot, "kept"], 4, w_sem(6, ("kept", slot)), dp=peer)
+                w_copy(slot, 6, parts[slot, "kept"], 4, w_sem(6, "kept"), dp=peer)
 
                 @pl.when(d % 2 == 1)
                 def _():
-                    w_copy(slot, 6, parts[slot, "moved"], 4, w_sem(6, ("moved", slot)), dp=peer)
+                    w_copy(slot, 6, parts[slot, "moved"], 4, w_sem(6, "moved"), dp=peer)
 
             into = w_sem(slot + 1, "second" if name == "second" else None)
             w_copy(slot, slot + 1, piece, 1, into, dp=core)
@@ -279,15 +288,15 @@
     def w_cross():
         @pl.when(d % 2 == 1)
         def _():
+            w_both(3, "second", half // 2)
             for slot in (2, 4):
-                arrived(w_ref(slot + 1, parts[slot, "second"]), w_sem(slot + 1, "second"))
-                w_copy(slot + 1, 7, parts[slot, "moved"], 4, w_sem(7, ("moved", slot)), dp=turns[slot][1])
+                w_copy(slot + 1, 7, parts[slot, "moved"], 4, w_sem(7, "moved"), dp=turns[slot][1])
 
     def w_lend():
         for giver, sends in (
             (0, [(2, "some", 1)]),
             (1, [(2, "lent", 0), (4, "lent", 0)]),
-            (2, [(2, "swap", 3), (4, "swap", 3), (4, "some", 1)]),
+            (2, [(2, "thin", 3), (4, "thin", 3), (4, "some", 1)]),
             (3, [(2, "swap", 2), (4, "swap", 2)]),
         ):
             @pl.when(z == giver)
@@ -296,85 +305,85 @@
                     w_copy(slot, slot, parts[slot, name], 5, w_sem(slot, "given"), sp=target)
 
     def w_diag(name):
+        part = "kept" if name == "second" else name
+        w_both(6, part, parts[2, part][1])
         for slot in (2, 4):
-            for part in ("first",) if name == "first" else ("kept",):
-                arrived(w_ref(6, parts[slot, part]), w_sem(6, (part, slot)))
-                w_copy(6, 7, parts[slot, part], 1, w_sem(7, None), dp=core)
+            w_copy(6, 7, parts[slot, part], 1, w_sem(7, None), dp=core)
         if name == "second":
             @pl.when(d % 2 == 1)
             def _():
+                w_both(6, "moved", shed)
                 for slot in (2, 4):
-                    piece = parts[slot, "moved"]
-                    arrived(w_ref(6, piece), w_sem(6, ("moved", slot)))
-                    w_copy(6, 7, piece, 1, w_sem(7, None), dp=core)
+                    w_copy(6, 7, parts[slot, "moved"], 1, w_sem(7, None), dp=core)
+                w_both(7, "moved", shed)
                 for slot in (2, 4):
-                    piece = parts[slot, "moved"]
-                    arrived(w_ref(7, piece), w_sem(7, ("moved", slot)))
-                    w_copy(7, 6, piece, 1, w_sem(6, ("moved", slot)), dp=core)
-
-    def w_arrived(slot):
-        if slot == 1:
-            arrived(w_buf.at[slot], w_sem(slot, None))
-            return
-        short = w_buf.at[slot, pl.ds(0, depth - 2 * shed)]
-        if slot == 7:
-            @pl.when(d % 2 == 0)
-            def _():
-                arrived(w_buf.at[slot], w_sem(slot, None))
-                for near in (2, 4):
-                    arrived(w_ref(6, parts[near, "moved"]), w_sem(6, ("moved", near)))
-
-            @pl.when(d % 2 == 1)
-            def _():
-                arrived(short, w_sem(slot, None))
-            return
-        arrived(short, w_sem(slot, None))
+                    w_copy(7, 6, parts[slot, "moved"], 1, w_sem(6, "moved"), dp=core)
+
+    def w_odd():
+        arrived(w_buf.at[pl.ds(0, 2), pl.ds(0, depth - 2 * shed)], w_sem(3, None))
 
         @pl.when(d % 2 == 0)
         def _():
-            arrived(w_ref(slot, parts[slot - 1, "second"]), w_sem(slot, "second"))
+            w_both(3, "second", half // 2)
+
+    def w_last():
+        @pl.when(d % 2 == 0)
+        def _():
+            arrived(w_buf.at[7], w_sem(7, None))
+            w_both(6, "moved", shed)
+
+        @pl.when(d % 2 == 1)
+        def _():
+            arrived(w_buf.at[7, pl.ds(0, depth - 2 * shed)], w_sem(7, None))
 
     local[0].wait()
     w_first()
-    for copy in local[1:]:
+    for copy in local[1:3]:
         copy.wait()
+    pltpu.make_async_copy(kv_own, kv_own, loc.at[3]).wait()
 
     for owner, target in ((0, 1), (1, 0), (1, 2), (2, 1), (2, 3), (3, 2)):
         @pl.when(z == owner)
         def _():
             gate_copy(owner, target).start()
 
+    def kv_start(start, stop):
+        for c in range(start, stop):
+            kv_copy(c).start()
+
+    def q_start(start, stop, slot, target):
+        for c in range(start, stop):
+            q_copy(c, slot, target).start()
+
     @pl.when(z == 0)
     def _():
-        for c in range(chunks):
-            kv_copy(c).start()
-            if c == 0:
-                pl.semaphore_wait(seen_sem.at[0], 1)
-                gate_copy(0, 2).start()
+        kv_start(0, 1)
+        pl.semaphore_wait(seen_sem, 1)
+        gate_copy(0, 2).start()
+        kv_start(1, chunks)
 
     @pl.when(z == HUB + 1)
     def _():
-        for c in range(chunks):
-            q_copy(c, 0, HUB).start()
-            if c == 0:
-                pl.semaphore_wait(seen_sem.at[0], 1)
-                gate_copy(2, 0).start()
+        q_start(0, 1, 0, HUB)
+        pl.semaphore_wait(seen_sem, 1)
+        gate_copy(2, 0).start()
+        q_start(1, chunks, 0, HUB)
 
     @pl.when(z == HUB + 2)
     def _():
-        q_copy(0, 1, HUB + 1).start()
-        pl.semaphore_wait(seen_sem.at[1], 1)
+        q_start(0, 1, 1, HUB + 1)
+        pl.semaphore_wait(seen_sem, 1)
         gate_copy(3, 1).start()
-        q_copy(0, 1, HUB).start()
-        q_copy(1, 1, HUB).start()
+        q_start(0, 1, 1, HUB)
+        q_start(1, 2, 1, HUB)
         for c in range(1, chunks):
-            q_copy(c, 1, HUB + 1).start()
+            q_start(c, c + 1, 1, HUB + 1)
             if c + 1 < chunks:
-                q_copy(c + 1, 1, HUB).start()
+                q_start(c + 1, c + 2, 1, HUB)
 
     @pl.when(z == HUB)
     def _():
-        pl.semaphore_wait(seen_sem.at[1], 1)
+        pl.semaphore_wait(seen_sem, 1)
         gate_copy(1, 3).start()
 
     @pl.when(z != HUB)
@@ -475,6 +484,19 @@
     cut = chunks // 2
     width = w_buf.shape[2]
 
+    def joined(c):
+        return JOINED[0] <= c < JOINED[1]
+
+    def runs(start, stop):
+        at = start
+        while at < stop:
+            end = at + 1
+            while end < stop and joined(end) == joined(at):
+                end += 1
+            yield at, end, joined(at)
+            at = end
+
+
     def product(slot, start, stop):
         span = pl.ds(start * LANES, (stop - start) * LANES)
         return jnp.dot(heads[:, span], w_buf[slot, span], preferred_element_type=jnp.float32)
@@ -496,7 +518,7 @@
             store(slot, total[n] + product(slot, start, chunks))
 
     def gather(stop):
-        w_arrived(1)
+        arrived(w_buf.at[1], w_sem(1, None))
         for n, slot in enumerate(EARLY):
             if stop == chunks:
                 project(slot)
@@ -531,17 +553,20 @@
 
     @pl.when(z == HUB)
     def _():
-        def hub(c, joined):
+        def far_give(c, joint):
+            if joint:
+                give(c, 1, 1, HUB + 1)
+            else:
+                give(c, 1, 0, HUB + 2)
+
+        def hub(c, joint):
             arrived(w_buf.at[0, pl.ds(0, 2 * rows)], in_rs.at[c])
             far, near, own = work(
                 c, [q_in.at[1], q_in.at[0], q_own], [HUB + 2, HUB + 1, HUB], True, [False, False, True]
             )
             put(c, 1, *far)
             put(c, 0, *near)
-            if joined:
-                give(c, 1, 1, HUB + 1)
-            else:
-                give(c, 1, 0, HUB + 2)
+            far_give(c, joint)
             give(c, 0, 0, HUB + 1)
             finish(c, own[0])
 
@@ -556,81 +581,102 @@
         hub_gates(range(HUB + 2, sp))
         arrived(w_buf.at[0, pl.ds(0, rows // 2)], in_rs.at[chunks])
         put(0, 1, *work(0, [q_in.at[1]], [HUB + 2], True, [False])[0])
-        give(0, 1, 0, HUB + 2)
+        far_give(0, joined(0))
         w_got("lent")
         w_lend()
 
-        @pl.loop(1, cut + 1)
-        def _(c):
-            on(c, 3, w_got, "first")
-            hub(c, True)
-
-        w_got("second")
-
-        @pl.loop(cut + 1, chunks)
-        def _(c):
-            @pl.when(c == chunks - 1)
-            def _():
-                w_got("bit")
-                w_cross()
-                w_diag("first")
-
-            hub(c, False)
+        for start, stop, joint in runs(1, chunks):
+            @pl.loop(start, stop)
+            def _(c):
+                on(c, 2 + d % 2, w_got, "first")
+                on(c, 4 + d % 2, w_got, "second")
+
+                @pl.when(c == chunks - 1)
+                def _():
+                    w_got("bit")
+                    w_cross()
+
+                    @pl.when(d % 2 == 1)
+                    def _():
+                        w_diag("first")
+
+                hub(c, joint)
+
+        @pl.when(d % 2 == 0)
+        def _():
+            w_diag("first")
 
         w_got("some")
         ends(chunks)
 
     @pl.when(z == HUB + 1)
     def _():
-        def near(c, joined):
+        def near(c, joint):
             arrived(q_in.at[1, :, cols(c)], in_rs.at[c])
             far, own = work(c, [q_in.at[1], q_own], [HUB + 2, HUB + 1], False, [False, True])
-            if joined:
-                o_far[c - 1], s_far[c - 1] = far
+            if joint:
+                o_far[c], s_far[c] = far
             else:
                 put(c, 1, *far)
                 give(c, 1, 1, HUB + 2)
             o_own[c], s_own[c] = own
 
-        def join(c, joined):
-            arrived(two_parts if joined else one_part, o_rs.at[c])
-            if joined:
-                put(c, 1, *merge((o_far[c - 1], s_far[c - 1]), (o_in[1, c], s_in[1, c])))
+        def join(c):
+            arrived(two_parts if joined(c) else one_part, o_rs.at[c])
+            if joined(c):
+                put(c, 1, *merge((o_far[c], s_far[c]), (o_in[1, c], s_in[1, c])))
                 give(c, 1, 1, HUB + 2)
             finish(c, merge((o_own[c], s_own[c]), (o_in[0, c], s_in[0, c]))[0])
 
-        near(0, False)
-
-        @pl.loop(1, cut + 1)
-        def _(c):
-            on(c, 3, w_got, "first")
-            near(c, True)
-
-        join(0, False)
-        join(1, True)
-
-        @pl.loop(cut + 1, chunks)
-        def _(c):
-            on(c, cut + 1, w_got, "second")
-
-            @pl.when(c == chunks - 1)
-            def _():
+        for start, stop, joint in runs(0, cut):
+            @pl.loop(start, stop)
+            def _(c):
+                on(c, 3, w_got, "first")
+                near(c, joint)
+
+        for c in range(cut, chunks):
+            join(c - cut)
+            if c == cut + 1:
+                w_got("second")
+            if c == chunks - 1:
+                join(cut)
                 w_got("rest")
                 w_cross()
-
-            near(c, False)
-            join(c - cut + 1, True)
-
+            near(c, joined(c))
         w_diag("first")
         w_got("given")
-
-        @pl.loop(cut + 1, chunks - 1)
-        def _(c):
-            join(c, False)
-
-        ends(chunks - 1)
-        join(chunks - 1, False)
-        remain(chunks - 1)
+        for c in range(chunks - 3, chunks - 2):
+            join(c)
+
+        @pl.when(d % 2 == 0)
+        def _():
+            w_diag("second")
+
+        join(chunks - 2)
+        gather(chunks - 1)
+
+        @pl.when(d % 2 == 1)
+        def _():
+            w_diag("second")
+
+        join(chunks - 1)
+        w_odd()
+
+        @pl.when(d % 2 == 0)
+        def _():
+            w_last()
+            remain(chunks - 1)
+            for slot in (3, 5, 6, 7):
+                project(slot)
+
+        @pl.when(d % 2 == 1)
+        def _():
+            remain(chunks - 1)
+            for slot in (3, 5):
+                project(slot)
+            w_last()
+            for slot in (6, 7):
+                project(slot)
 
     @pl.when(z == HUB + 2)
     def _():
@@ -640,56 +686,47 @@
                 c = 2 * pair + n
                 o_own[c], s_own[c] = work(c, [q_own], [z], False, [True])[0]
 
-        def join(c, joined):
-            arrived(one_part if joined else two_parts, o_rs.at[c])
+        def join(c):
+            arrived(one_part if joined(c) else two_parts, o_rs.at[c])
             pieces = [(o_own[c], s_own[c]), (o_in[1, c], s_in[1, c])]
-            if not joined:
+            if not joined(c):
                 pieces.append((o_in[0, c], s_in[0, c]))
             finish(c, merge(*pieces)[0])
 
         w_got("first")
         w_got("second")
-        w_got("rest")
+        w_got("most")
         w_cross()
         w_diag("first")
-        w_got("given")
-        join(0, False)
-
-        @pl.loop(1, cut - 1)
-        def _(c):
-            join(c, True)
+        w_got("thin")
+        for c in range(cut - 1):
+            join(c)
 
         @pl.when(d % 2 == 0)
         def _():
             w_diag("second")
 
-        join(cut - 1, True)
+        join(cut - 1)
         gather(cut)
 
         @pl.when(d % 2 == 1)
         def _():
             w_diag("second")
 
-        join(cut, True)
-
-        @pl.loop(cut + 1, chunks)
-        def _(c):
-            join(c, False)
-
-        w_arrived(3)
-        w_arrived(5)
-        w_arrived(7)
+        for c in range(cut, chunks):
+            join(c)
+        w_odd()
+        w_last()
         remain(cut)
         for slot in (3, 5, 6, 7):
             project(slot)
 
-    @pl.when(z <= HUB + 1)
-    def _():
-        for slot in (3, 5):
-            w_arrived(slot)
+    @pl.when(z <= HUB)
+    def _():
+        w_odd()
         for slot in (3, 5):
             project(slot)
-        w_arrived(7)
+        w_last()
         for slot in (6, 7):
             project(slot)
 
@@ -701,13 +738,13 @@
             for plane in range(sp):
                 @pl.when(z == plane)
                 def _():
-                    each = 5 * depth // 8 + (0, shed // 4, shed // 2, shed // 2)[plane] + moved // 2
+                    each = 5 * depth // 8 + (0, shed // 4, shed // 2, shed - THIN * shed // 8)[plane] + moved // 2
                     sent(w_buf.at[pl.ds(0, 4), pl.ds(0, each)], snd.at[4])
 
-    for giver, count in enumerate((3, 8, 7, 4)):
+    for giver, count in enumerate((6, 16, 6 + 2 * THIN, 8)):
         @pl.when(z == giver)
         def _():
-            sent(w_buf.at[0, pl.ds(0, count * shed // 2)], snd.at[5])
+            sent(w_buf.at[0, pl.ds(0, count * shed // 4)], snd.at[5])
 
     @pl.when((z == 0) | (z == HUB + 2))
     def _():
@@ -760,15 +797,15 @@
             pltpu.VMEM((2, chunks, 2, rows), f32),
             pltpu.VMEM((chunks, LANES, rows), f32),
             pltpu.VMEM((chunks, 2, rows), f32),
-            pltpu.VMEM((chunks // 2, LANES, rows), f32),
-            pltpu.VMEM((chunks // 2, 2, rows), f32),
+            pltpu.VMEM((chunks, LANES, rows), f32),
+            pltpu.VMEM((chunks, 2, rows), f32),
             pltpu.VMEM((len(EARLY), rows, block), f32),
             pltpu.VMEM((rows, width), bf16),
             pltpu.VMEM((dp, depth, block), bf16),
             pltpu.VMEM((LANES // 4 + 1, 2, rows), f32),
             pltpu.VMEM((LANES // 2 + 2, 2, rows), f32),
-            dma((chunks + 1,)), dma((chunks,)), dma((6,)), dma((2,)), dma((2,)), dma((24,)), dma((5,)),
-            pltpu.SemaphoreType.REGULAR((2,)),
+            dma((chunks + 1,)), dma((chunks,)), dma((6,)), dma((2,)), dma((2,)), dma((13,)), dma((4,)),
+            pltpu.SemaphoreType.REGULAR,
         ],
         compiler_params=pltpu.CompilerParams(collective_id=0, has_side_effects=True, vmem_limit_bytes=16 * 2**20),
         name="layer",

time: 22.7 us -> 22.3 us (0.982)
  the two profiles are of different devices: /device:TPU:19 before, /device:TPU:25 now
where the time goes in v3:
time: 22.3 us; the launch traced here: 22.2 us
  Pallas kernels  21.4 us (96%)
  local copies, waits for them, and re-layouts  0.8 us (4%)
    pallas_call x1, Pallas kernels, fused_shards(): pl.pallas_call(functools.partial(layer_kernel, (sp, chunks, head_size, he...  21.4 us
    unnamed x1, local copies, waits for them, and re-layouts  0.8 us

profile of v3, /device:TPU:25, one launch (start us, length us, event | category | flops | bytes accessed | tf_op | source)
XLA Modules:
  0.0 22.2 jit_solution(7101192379984255188)
XLA Ops:
  0.0 21.4 %layer.1 = bf16[1,128,2048]{2,1,0:T(8,128)(2,1)S(1)} custom-call(bf16[1,128,1024]{2,1,0:T(8,128)(2,1)} %q_hbm.1, bf16[1,128,1024]{2,1,0:T(8,128)(2,1)} %k_hbm.1, bf16[1,128,1024]{2,1,0:T(8,128)(2,1)} %v_hbm.1, f32[1,4,512]{2,1,0:T(4,128)} %g_hbm.1, bf16[1024,256]{1,0:T(8,128)(2,1)} %w_hbm.1), custom_call_target="tpu_custom_call" | custom-call | tf_op jit(solution)/shard_map/layer/pallas_call | solution.py:780
  21.4 0.8 %copy.7 = bf16[1,128,2048]{2,1,0:T(8,128)(2,1)} copy(bf16[1,128,2048]{2,1,0:T(8,128)(2,1)S(1)} %layer.1) | data formatting | bytes 1048576
